TPU v7x, 512 devices: a 8x2x16 block of a 8x8x16 slice. The times are simulated.
512 devices in a mesh: grp: 2 (over y), dp: 8 (over x), kv: 16 (over z), tp: 2 (over core).
Axes of the slice: x: 8, y: 2, z: 16, core: 2. Of those that a mesh axis runs over, the one named last changes fastest.
The devices are a block of a 8x8x16 slice.
Arguments:
- inputs: bfloat16 [512, 4096], P(('grp', 'dp'), 'kv'), parts along dimension 0, may hold values from -6 to 6
- gain_in: float32 [4096], P('kv'), may hold values from 0.1 to 1.9
- w_gate: bfloat16 [4096, 2048], P('kv', 'tp'), may hold values from -0.09375 to 0.09375
- w_input: bfloat16 [4096, 2048], P('kv', 'tp'), may hold values from -0.09375 to 0.09375
- w_bproj: bfloat16 [4096, 1024], P('kv', 'tp'), may hold values from -0.09375 to 0.09375
- w_cproj: bfloat16 [4096, 1024], P('kv', 'tp'), may hold values from -0.09375 to 0.09375
- w_step: bfloat16 [4096, 32], P('kv', 'tp'), may hold values from -0.09375 to 0.09375
- conv_input: float32 [4, 2048], P(None, 'tp'), may hold values from -3 to 3
- conv_bproj: float32 [4, 1024], P(None, 'tp'), may hold values from -3 to 3
- conv_cproj: float32 [4, 1024], P(None, 'tp'), may hold values from -3 to 3
- tail_input: bfloat16 [512, 3, 2048], P(('grp', 'dp', 'kv'), None, 'tp'), parts along dimension 0, may hold values from -6 to 6
- tail_bproj: bfloat16 [512, 3, 1024], P(('grp', 'dp', 'kv'), None, 'tp'), parts along dimension 0, may hold values from -6 to 6
- tail_cproj: bfloat16 [512, 3, 1024], P(('grp', 'dp', 'kv'), None, 'tp'), parts along dimension 0, may hold values from -6 to 6
- step_bias: float32 [32], P('tp'), may hold values from -3 to 0
- decay_log: float32 [32], P('tp'), may hold values from -2 to 2
- block_input: bfloat16 [512, 128, 2048], P(('grp', 'dp', 'kv'), None, 'tp'), parts along dimension 0, may hold values from -6 to 6
- block_bproj: bfloat16 [512, 128, 1024], P(('grp', 'dp', 'kv'), None, 'tp'), parts along dimension 0, may hold values from -0.59765625 to 0.59765625
- block_step: float32 [512, 128, 32], P(('grp', 'dp', 'kv'), None, 'tp'), parts along dimension 0, may hold values from 0.005 to 0.2
- lengths: int32 [512], P(('grp', 'dp', 'kv')), parts along dimension 0, may hold values from 1 to 127, 8192 in all
- state: float32 [512, 32, 64, 128], P(('grp', 'dp', 'kv'), 'tp'), parts along dimension 0, may hold values from -0.6 to 0.6
- gain_mix: float32 [2048], P('tp'), may hold values from 0.1 to 1.9
- w_out: bfloat16 [2048, 4096], P('tp', 'kv'), may hold values from -0.125 to 0.125
- gain_mlp: float32 [4096], P(('kv', 'tp')), may hold values from 0.1 to 1.9
- w_up: bfloat16 [4096, 16384], P(('kv', 'tp'), 'dp'), may hold values from -0.09375 to 0.09375
- w_down: bfloat16 [16384, 4096], P('dp', ('kv', 'tp')), may hold values from -0.046875 to 0.046875
Outputs:
- layer_out: bfloat16 [512, 4096], P(('grp', 'dp'), ('kv', 'tp')), parts along dimension 0
There are 2 independent parts, one for each index of `grp`. A program takes and returns all parts, laid end to end along the dimension named above; an argument that names none is the same for every part. Nothing has to cross between parts.
Inputs may be any that keep to these rules, and one draw needn't show every extreme that they name: `lengths`: the number of live positions before the new token in each sequence's current block; the largest equals 127 in every draw.
All inputs are finite; a program needn't handle non-finite values.
Results may differ from a plain program's by a relative error of at most 0.012.
Values may be sent and summed in bfloat16 or wider, within the bound.
No kernel may reach another device: no remote copies, remote signals or barrier semaphores. Data moves between devices by JAX's collectives and lax.ppermute only.
A program may use at most 64 MiB of HBM per device.

v0:
```python
import math
import jax
import jax.numpy as jnp
from jax import lax
from jax.sharding import PartitionSpec as P

D = 4096
HEAD_DIM = 64
D_STATE = 128
TAPS = 4
SSM_WIDTH = 2048
EPS = 1e-06


def in_blocks(shard, dim, size):
    before, after = (shard.shape[:dim], shard.shape[dim + 1 :])
    return jnp.moveaxis(shard.reshape(*before, size, -1, *after), dim, 0)


def sent_and_summed(shard, axis, dim):
    size = lax.axis_size(axis)
    tiles = lax.all_to_all(in_blocks(shard, dim, size), axis, 0, 0, tiled=True)
    return jnp.sum(tiles, axis=0)


def sent_together(arrays, axis, dim, along):
    widths = [math.prod(a.shape[along:]) for a in arrays]
    both = jnp.concatenate(
        [a.reshape(*a.shape[:along], w) for a, w in zip(arrays, widths)], axis=along
    )
    whole = sent_and_summed(both, axis, dim)
    tiles = jnp.split(whole, [sum(widths[:k]) for k in range(1, len(widths))], axis=along)
    return tuple((b.reshape(*whole.shape[:along], *a.shape[along:]) for a, b in zip(arrays, tiles)))


def gathered_total(shard, axis):
    return lax.all_gather(shard, axis).sum(0)


def from_everyone(shard, axis):
    size = lax.axis_size(axis)
    return lax.all_to_all(
        jnp.broadcast_to(shard[None], (size, *shard.shape)), axis, 0, 0, tiled=True
    )


def joined_along(tiles, dim):
    dims = list(tiles.shape[1:])
    dims[dim] *= tiles.shape[0]
    return jnp.moveaxis(tiles, 0, dim).reshape(dims)


def gather_directly(shard, axis, dim):
    tiles = from_everyone(shard, axis)
    return joined_along(tiles, dim)


def in_one_piece(arrays, axis, dim, along):
    ends, at = ([], 0)
    for a in arrays[:-1]:
        at += a.shape[along]
        ends.append(at)
    both = jnp.concatenate(arrays, axis=along)
    return tuple(jnp.split(lax.all_gather(both, axis, axis=dim, tiled=True), ends, axis=along))


def of_everyone(shard, axis):
    everything = from_everyone(shard, axis)
    return jnp.sum(everything, axis=0)


def summed_on_arrival(shard, axis, dim):
    tiles = in_blocks(shard, dim, lax.axis_size(axis))
    arrived = lax.all_to_all(tiles, axis, split_axis=0, concat_axis=0, tiled=True)
    return arrived.astype(jnp.float32).sum(axis=0)


def stacked_from(shard, axes, order):
    tiles = shard[None]
    for k in order:
        tiles = lax.all_gather(tiles, axes[k], axis=0, tiled=True)
    current = [lax.axis_size(axes[k]) for k in reversed(order)]
    tiles = tiles.reshape(*current, *shard.shape)
    turned = sorted(range(len(order)), key=lambda place: order[len(order) - 1 - place])
    return tiles.transpose(*turned, *range(len(order), tiles.ndim)).reshape(-1, *shard.shape)


def gathered_by_axis(shard, axes, order, dim):
    return joined_along(stacked_from(shard, axes, order), dim)


def convolve(history, weights, newest):
    summed = weights[TAPS - 1] * newest
    for offset in range(TAPS - 1):
        summed = summed + weights[offset] * history[:, offset].astype(jnp.float32)
    return jax.nn.silu(summed)


def per_device(
    inputs,
    gain_in,
    w_gate,
    w_input,
    w_bproj,
    w_cproj,
    w_step,
    conv_input,
    conv_bproj,
    conv_cproj,
    tail_input,
    tail_bproj,
    tail_cproj,
    step_bias,
    decay_log,
    block_input,
    block_bproj,
    block_step,
    lengths,
    state,
    gain_mix,
    w_out,
    gain_mlp,
    w_up,
    w_down,
):
    stream = inputs.astype(jnp.float32)
    squares = jnp.sum(stream * stream, axis=1)
    scaled = (stream * gain_in).astype(jnp.bfloat16)
    matrices = (w_gate, w_input, w_bproj, w_cproj, w_step)
    pieces = [jnp.dot(scaled, weight, preferred_element_type=jnp.float32) for weight in matrices]
    projected, totals = sent_together((jnp.concatenate(pieces, axis=1), squares), "kv", 0, 1)
    inverse = lax.rsqrt(totals / D + EPS)[:, None]
    bounds = [0]
    for weight in matrices:
        bounds.append(bounds[-1] + weight.shape[1])
    gate_pre, value_pre, b_pre, c_pre, step_pre = [
        projected[:, bounds[member] : bounds[member + 1]] * inverse for member in range(5)
    ]
    seq_count = lengths.shape[0]
    head_count = step_bias.shape[0]
    group_count = w_bproj.shape[1] // D_STATE
    block_len = block_step.shape[1]
    per_group = head_count // group_count
    current = convolve(tail_input, conv_input, value_pre)
    b_now = convolve(tail_bproj, conv_bproj, b_pre)
    c_now = convolve(tail_cproj, conv_cproj, c_pre)
    step_size = jax.nn.softplus(step_pre + step_bias)
    decay_rate = -jnp.exp(decay_log)
    positions = lax.broadcasted_iota(jnp.int32, (1, block_len), 1)
    live_rows = (positions < lengths[:, None]).astype(jnp.float32)
    masked = block_step * live_rows[:, :, None]
    later_steps = jnp.sum(masked, axis=1, keepdims=True) - jnp.cumsum(masked, axis=1)
    decays = jnp.exp(decay_rate * (step_size[:, None, :] + later_steps)) * live_rows[:, :, None]
    c_query = c_now.astype(jnp.bfloat16).reshape(seq_count, group_count, D_STATE)
    keys = block_bproj.reshape(seq_count, block_len, group_count, D_STATE)
    scores = jnp.einsum("bsgn,bgn->bsg", keys, c_query, preferred_element_type=jnp.float32)
    scores = jnp.repeat(scores, per_group, axis=2)
    weights = (decays * scores * block_step).astype(jnp.bfloat16)
    values = block_input.reshape(seq_count, block_len, head_count, HEAD_DIM)
    inner_sum = jnp.einsum("bsh,bshp->bhp", weights, values, preferred_element_type=jnp.float32)
    c_full = c_now.reshape(seq_count, group_count, D_STATE)
    b_full = b_now.reshape(seq_count, group_count, D_STATE)
    own_score = jnp.repeat(jnp.sum(c_full * b_full, axis=2), per_group, axis=1)
    own_term = (step_size * own_score)[:, :, None] * current.reshape(
        seq_count, head_count, HEAD_DIM
    )
    carried = jnp.exp(decay_rate * (step_size + jnp.sum(masked, axis=1)))
    c_heads = jnp.repeat(c_full, per_group, axis=1)
    readout = jnp.einsum("bhpn,bhn->bhp", state, c_heads, precision=lax.Precision.HIGHEST)
    mixed = (inner_sum + own_term + carried[:, :, None] * readout).reshape(
        seq_count, -1
    ) * jax.nn.silu(gate_pre)
    local_sq = jnp.sum(mixed * mixed, axis=1)
    total_sq = gathered_total(local_sq, "tp")
    normed = (mixed * lax.rsqrt(total_sq / SSM_WIDTH + EPS)[:, None] * gain_mix).astype(
        jnp.bfloat16
    )
    products = jnp.dot(gather_directly(normed, "kv", 0), w_out, preferred_element_type=jnp.float32)
    mixed_in = sent_and_summed(products, "tp", 1)
    column_count = mixed_in.shape[1]
    residual = lax.dynamic_slice_in_dim(
        stream, lax.axis_index("tp") * column_count, column_count, 1
    )
    hidden = (residual + mixed_in).astype(jnp.bfloat16)
    lifted = (hidden.astype(jnp.float32) * gain_mlp).astype(jnp.bfloat16)
    all_lifted, all_hidden = in_one_piece((lifted, hidden), "dp", 0, 1)
    whole_rows = all_hidden.astype(jnp.float32)
    row_sq = jnp.sum(whole_rows * whole_rows, axis=1)
    partial_value = jnp.dot(all_lifted, w_up, preferred_element_type=jnp.float32)
    sq_sum = of_everyone(row_sq, ("kv", "tp"))
    shares = summed_on_arrival(partial_value.astype(jnp.bfloat16), ("kv", "tp"), 1)
    unit_share = jnp.square(jax.nn.relu(shares * lax.rsqrt(sq_sum / D + EPS)[:, None])).astype(
        jnp.bfloat16
    )
    hidden_units = gathered_by_axis(unit_share, ("kv", "tp"), (0, 1), 1)
    lowered = sent_and_summed(
        jnp.dot(hidden_units, w_down, preferred_element_type=jnp.float32), "dp", 0
    )
    return (hidden.astype(jnp.float32) + lowered).astype(jnp.bfloat16)


def solution(mesh):
    return jax.shard_map(
        per_device,
        mesh=mesh,
        in_specs=(
            P(("grp", "dp"), "kv"),
            P("kv"),
            P("kv", "tp"),
            P("kv", "tp"),
            P("kv", "tp"),
            P("kv", "tp"),
            P("kv", "tp"),
            P(None, "tp"),
            P(None, "tp"),
            P(None, "tp"),
            P(("grp", "dp", "kv"), None, "tp"),
            P(("grp", "dp", "kv"), None, "tp"),
            P(("grp", "dp", "kv"), None, "tp"),
            P("tp"),
            P("tp"),
            P(("grp", "dp", "kv"), None, "tp"),
            P(("grp", "dp", "kv"), None, "tp"),
            P(("grp", "dp", "kv"), None, "tp"),
            P(("grp", "dp", "kv")),
            P(("grp", "dp", "kv"), "tp", None, None),
            P("tp"),
            P("tp", "kv"),
            P(("kv", "tp")),
            P(("kv", "tp"), "dp"),
            P("dp", ("kv", "tp")),
        ),
        out_specs=P(("grp", "dp"), ("kv", "tp")),
        check_vma=False,
    )
```

profile of v0, /device:TPU:65, one launch (start us, length us, event | category | flops | bytes accessed | tf_op | source)
XLA Modules:
  0.0 298.7 jit_solution(5687502616347760678)
XLA Ops:
  6.6 0.9 multiply_reduce_fusion.1
  7.5 0.1 concatenate.27
  7.6 0.9 fusion.14
  8.5 1.1 fusion.16
  9.7 1.2 fusion.15
  10.9 1.3 fusion.18
  12.3 0.9 fusion.17
  13.4 1.2 concatenate.25
  14.6 44.4 %all-to-all-start = ((f32[16,2,3089]{2,1,0:T(2,128)}), f32[16,2,3089]{2,1,0:T(2,128)S(1)}, u32[]{:S(2)}, u32[]{:S(2)}) async-start(f32[16,2,3089]{2,1,0:T(2,128)} %concatenate.25), calls=%async_computation | async-start | bytes 819200 | tf_op jit(solution)/shard_map/all_to_all | solution.py:22
  59.1 0.2 copy.88
  59.3 1.0 copy.74
  60.3 1.3 dynamic-slice
  62.3 0.1 fusion.33
  62.4 0.2 reduce_window_sum.11
  62.7 15.6 %all-to-all-done = f32[16,2,3089]{2,1,0:T(2,128)S(1)} async-done(((f32[16,2,3089]{2,1,0:T(2,128)}), f32[16,2,3089]{2,1,0:T(2,128)S(1)}, u32[]{:S(2)}, u32[]{:S(2)}) %all-to-all-start) | async-done | bytes 395424 | tf_op jit(solution)/shard_map/all_to_all | solution.py:22
  78.3 0.1 reduce_sum.106
  78.5 0.2 fusion.30
  79.2 0.2 fusion.38
  79.6 0.1 fusion.2
  79.9 1.7 fusion.40
  81.6 1.4 fusion.39
  83.2 0.2 multiply_reduce_fusion.2
  83.4 0.2 dynamic-update-slice
  83.7 8.0 %all-reduce = f32[4]{0:T(128)S(1)} all-reduce(f32[4]{0:T(128)S(1)} %dynamic-update-slice), channel_id=2, replica_groups=mesh['grp'=2,'dp'=8,'kv'=16,'tp'=2] {'tp'}, use_global_device_ids=true, to_apply=%add | all-reduce | flops 4 | bytes 32
  91.8 0.7 broadcast_in_dim.13
  92.5 6.0 %all-to-all-start.1 = ((bf16[16,2,1024]{2,1,0:T(2,128)(2,1)}), bf16[16,2,1024]{2,1,0:T(2,128)(2,1)S(1)}, u32[]{:S(2)}, u32[]{:S(2)}) async-start(bf16[16,2,1024]{2,1,0:T(2,128)(2,1)} %broadcast_in_dim.13), calls=%async_computation.1 | async-start | bytes 131072 | tf_op jit(solution)/shard_map/all_to_all | solution.py:42
  98.5 0.2 copy.89
  98.7 11.2 %all-to-all-done.1 = bf16[16,2,1024]{2,1,0:T(2,128)(2,1)S(1)} async-done(((bf16[16,2,1024]{2,1,0:T(2,128)(2,1)}), bf16[16,2,1024]{2,1,0:T(2,128)(2,1)S(1)}, u32[]{:S(2)}, u32[]{:S(2)}) %all-to-all-start.1) | async-done | bytes 65568 | tf_op jit(solution)/shard_map/all_to_all | solution.py:42
  110.0 0.2 convolution_bitcast_fusion
  110.2 5.5 %all_to_all.31 = f32[2,32,128]{2,1,0:T(8,128)S(1)} all-to-all(f32[2,32,128]{2,1,0:T(8,128)S(1)} %convolution_bitcast_fusion), channel_id=1, replica_groups=mesh['grp'=2,'dp'=8,'kv'=16,'tp'=2] {'tp'}, dimensions={0} | all-to-all | bytes 65536 | tf_op jit(solution)/shard_map/all_to_all | solution.py:22
  115.7 20.2 %all_gather.17 = bf16[256,256]{1,0:T(8,128)(2,1)S(1)} all-gather(bf16[32,256]{1,0:T(8,128)(2,1)S(1)} %pad_maximum_fusion), channel_id=1, replica_groups=mesh['grp'=2,'dp'=8,'kv'=16,'tp'=2] {'dp'}, dimensions={0}, use_global_device_ids=true | all-gather | bytes 147456 | tf_op jit(solution)/shard_map/all_gather | solution.py:64
  135.9 0.1 multiply_reduce_fusion
  136.0 0.6 broadcast_in_dim.14
  136.6 10.4 %all-to-all-start.4 = ((f32[32,1,256]{2,1,0:T(1,128)}), f32[32,1,256]{2,1,0:T(1,128)S(1)}, u32[]{:S(2)}, u32[]{:S(2)}) async-start(f32[32,1,256]{2,1,0:T(1,128)} %broadcast_in_dim.14), calls=%async_computation.4 | async-start | bytes 65536 | tf_op jit(solution)/shard_map/all_to_all | solution.py:42
  147.1 0.4 convolution_convert_fusion
  147.5 1.3 copy.76
  148.8 10.4 %all-to-all-done.4 = f32[32,1,256]{2,1,0:T(1,128)S(1)} async-done(((f32[32,1,256]{2,1,0:T(1,128)}), f32[32,1,256]{2,1,0:T(1,128)S(1)}, u32[]{:S(2)}, u32[]{:S(2)}) %all-to-all-start.4) | async-done | bytes 32800 | tf_op jit(solution)/shard_map/all_to_all | solution.py:42
  159.2 4.8 %all-to-all-start.3 = ((bf16[32,256,64]{1,2,0:T(8,128)(2,1)}), bf16[32,256,64]{1,2,0:T(8,128)(2,1)S(1)}, u32[]{:S(2)}, u32[]{:S(2)}) async-start(bf16[32,256,64]{1,2,0:T(8,128)(2,1)} %bitcast.41), calls=%async_computation.3 | async-start | bytes 2097152 | tf_op jit(solution)/shard_map/all_to_all | solution.py:74
  164.2 55.5 %all-to-all-done.3 = bf16[32,256,64]{1,2,0:T(8,128)(2,1)S(1)} async-done(((bf16[32,256,64]{1,2,0:T(8,128)(2,1)}), bf16[32,256,64]{1,2,0:T(8,128)(2,1)S(1)}, u32[]{:S(2)}, u32[]{:S(2)}) %all-to-all-start.3) | async-done | bytes 1048608 | tf_op jit(solution)/shard_map/all_to_all | solution.py:74
  219.7 0.2 convert_reduce_fusion
  219.8 24.8 %all_gather.18 = bf16[16,256,64]{1,2,0:T(8,128)(2,1)} all-gather(bf16[1,256,64]{1,2,0:T(8,128)(2,1)S(1)} %fusion.6), channel_id=1, replica_groups=mesh['grp'=2,'dp'=8,'kv'=16,'tp'=2] {'kv'}, dimensions={0}, use_global_device_ids=true | all-gather | bytes 557056 | tf_op jit(solution)/shard_map/all_gather | solution.py:81
  244.7 23.7 %all-gather.3.cloned.1.call-done = bf16[32,256,64]{1,2,0:T(8,128)(2,1)} async-done(((bf16[16,256,64]{1,2,0:T(8,128)(2,1)}), bf16[32,256,64]{1,2,0:T(8,128)(2,1)}) %all-gather.3.cloned.1.call-update) | async-done | bytes 1048592 | tf_op jit(solution)/shard_map/all_gather | solution.py:81
  268.5 2.4 copy.78
  270.8 3.9 %copy.79 = bf16[256,32,64]{2,1,0:T(8,128)(2,1)S(1)} copy(bf16[256,32,64]{0,2,1:T(8,128)(2,1)} %bitcast.101) | data formatting | bytes 2097152 | tf_op jit(solution)/shard_map/transpose | solution.py:50
  274.7 2.4 dot_general.51
  277.2 1.8 fusion
  279.0 12.3 %all_to_all.32 = f32[8,32,128]{2,1,0:T(8,128)S(1)} all-to-all(f32[8,32,128]{2,1,0:T(8,128)S(1)} %fusion), channel_id=1, replica_groups=mesh['grp'=2,'dp'=8,'kv'=16,'tp'=2] {'dp'}, dimensions={0} | all-to-all | bytes 262144 | tf_op jit(solution)/shard_map/all_to_all | solution.py:22
  291.3 0.6 fusion.8
  (81 shorter events, 2.0 us)
Async XLA Ops:
  6.5 73.3 %copy-start = (f32[2,16,64,128]{3,2,1,0:T(8,128)S(1)}, f32[2,16,64,128]{3,2,1,0:T(8,128)}, u32[]{:S(2)}) copy-start(f32[2,16,64,128]{3,2,1,0:T(8,128)} %param.44) | copy-start | bytes 3145732
  6.6 5.8 %copy-start.3 = (bf16[256,1024]{1,0:T(8,128)(2,1)S(1)}, bf16[256,1024]{1,0:T(8,128)(2,1)}, u32[]{:S(2)}) copy-start(bf16[256,1024]{1,0:T(8,128)(2,1)} %param.28) | copy-start | bytes 1572868
  9.6 49.4 %copy-start.7 = (f32[2,128,16]{1,2,0:T(8,128)S(1)}, f32[2,128,16]{1,2,0:T(8,128)}, u32[]{:S(2)}) copy-start(f32[2,128,16]{1,2,0:T(8,128)} %param.42) | copy-start | bytes 49156
  9.7 49.4 %copy-start.6 = (bf16[2,128,512]{2,1,0:T(8,128)(2,1)S(1)}, bf16[2,128,512]{2,1,0:T(8,128)(2,1)}, u32[]{:S(2)}) copy-start(bf16[2,128,512]{2,1,0:T(8,128)(2,1)} %param.41) | copy-start | bytes 786436
  10.9 48.4 %copy-start.4 = (bf16[2,128,1024]{2,1,0:T(8,128)(2,1)S(1)}, bf16[2,128,1024]{2,1,0:T(8,128)(2,1)}, u32[]{:S(2)}) copy-start(bf16[2,128,1024]{2,1,0:T(8,128)(2,1)} %param.40) | copy-start | bytes 1572868
  12.3 49.9 %copy-start.17 = (s32[2]{0:T(128)S(1)}, s32[2]{0:T(128)}, u32[]{:S(2)}) copy-start(s32[2]{0:T(128)} %param.43) | copy-start | bytes 28
  13.3 49.3 %copy-start.18 = (f32[16]{0:T(128)S(1)}, f32[16]{0:T(128)}, u32[]{:S(2)}) copy-start(f32[16]{0:T(128)} %param.39) | copy-start | bytes 196
  13.3 49.3 %copy-start.10 = (f32[4,512]{1,0:T(4,128)S(1)}, f32[4,512]{1,0:T(4,128)}, u32[]{:S(2)}) copy-start(f32[4,512]{1,0:T(4,128)} %param.33) | copy-start | bytes 24580
  13.3 49.3 %copy-start.11 = (f32[4,512]{1,0:T(4,128)S(1)}, f32[4,512]{1,0:T(4,128)}, u32[]{:S(2)}) copy-start(f32[4,512]{1,0:T(4,128)} %param.34) | copy-start | bytes 24580
  13.3 49.3 %copy-start.8 = (f32[4,1024]{1,0:T(4,128)S(1)}, f32[4,1024]{1,0:T(4,128)}, u32[]{:S(2)}) copy-start(f32[4,1024]{1,0:T(4,128)} %param.32) | copy-start | bytes 49156
  13.4 65.2 %copy-start.12 = (bf16[2,3,512]{2,0,1:T(2,128)(2,1)S(1)}, bf16[2,3,512]{2,0,1:T(2,128)(2,1)}, u32[]{:S(2)}) copy-start(bf16[2,3,512]{2,0,1:T(2,128)(2,1)} %param.37) | copy-start | bytes 18436
  13.4 65.2 %copy-start.13 = (bf16[2,3,512]{2,0,1:T(2,128)(2,1)S(1)}, bf16[2,3,512]{2,0,1:T(2,128)(2,1)}, u32[]{:S(2)}) copy-start(bf16[2,3,512]{2,0,1:T(2,128)(2,1)} %param.36) | copy-start | bytes 18436
  13.4 65.6 %copy-start.9 = (bf16[2,3,1024]{2,0,1:T(2,128)(2,1)S(1)}, bf16[2,3,1024]{2,0,1:T(2,128)(2,1)}, u32[]{:S(2)}) copy-start(bf16[2,3,1024]{2,0,1:T(2,128)(2,1)} %param.35) | copy-start | bytes 36868
  14.6 64.9 %copy-start.16 = (f32[16]{0:T(128)S(1)}, f32[16]{0:T(128)}, u32[]{:S(2)}) copy-start(f32[16]{0:T(128)} %param.38) | copy-start | bytes 196
  14.6 63.7 %all-to-all-start = ((f32[16,2,3089]{2,1,0:T(2,128)}), f32[16,2,3089]{2,1,0:T(2,128)S(1)}, u32[]{:S(2)}, u32[]{:S(2)}) async-start(f32[16,2,3089]{2,1,0:T(2,128)} %concatenate.25), calls=%async_computation | async-start | bytes 819200 | tf_op jit(solution)/shard_map/all_to_all | solution.py:22
  60.3 31.5 %copy-start.14 = (f32[1024]{0:T(1024)S(1)}, f32[1024]{0:T(1024)}, u32[]{:S(2)}) copy-start(f32[1024]{0:T(1024)} %param.45) | copy-start | bytes 12292
  62.3 36.2 %copy-start.1 = (bf16[32,256]{1,0:T(8,128)(2,1)S(1)}, bf16[32,256]{1,0:T(8,128)(2,1)}, u32[]{:S(2)}) copy-start(bf16[32,256]{1,0:T(8,128)(2,1)} %param.25) | copy-start | bytes 49156
  62.4 36.1 %copy-start.5 = (bf16[1024,256]{1,0:T(8,128)(2,1)S(1)}, bf16[1024,256]{1,0:T(8,128)(2,1)}, u32[]{:S(2)}) copy-start(bf16[1024,256]{1,0:T(8,128)(2,1)} %param.46) | copy-start | bytes 1572868
  79.8 35.9 %copy-start.15 = (f32[128]{0:T(128)S(1)}, f32[128]{0:T(128)}, u32[]{:S(2)}) copy-start(f32[128]{0:T(128)} %param.47) | copy-start | bytes 1540
  79.9 67.2 %copy-start.2 = (bf16[128,2048]{1,0:T(8,128)(2,1)S(1)}, bf16[128,2048]{1,0:T(8,128)(2,1)}, u32[]{:S(2)}) copy-start(bf16[128,2048]{1,0:T(8,128)(2,1)} %param.48) | copy-start | bytes 1572868
  92.5 17.4 %all-to-all-start.1 = ((bf16[16,2,1024]{2,1,0:T(2,128)(2,1)}), bf16[16,2,1024]{2,1,0:T(2,128)(2,1)S(1)}, u32[]{:S(2)}, u32[]{:S(2)}) async-start(bf16[16,2,1024]{2,1,0:T(2,128)(2,1)} %broadcast_in_dim.13), calls=%async_computation.1 | async-start | bytes 131072 | tf_op jit(solution)/shard_map/all_to_all | solution.py:42
  136.6 22.6 %all-to-all-start.4 = ((f32[32,1,256]{2,1,0:T(1,128)}), f32[32,1,256]{2,1,0:T(1,128)S(1)}, u32[]{:S(2)}, u32[]{:S(2)}) async-start(f32[32,1,256]{2,1,0:T(1,128)} %broadcast_in_dim.14), calls=%async_computation.4 | async-start | bytes 65536 | tf_op jit(solution)/shard_map/all_to_all | solution.py:42
  159.2 60.5 %all-to-all-start.3 = ((bf16[32,256,64]{1,2,0:T(8,128)(2,1)}), bf16[32,256,64]{1,2,0:T(8,128)(2,1)S(1)}, u32[]{:S(2)}, u32[]{:S(2)}) async-start(bf16[32,256,64]{1,2,0:T(8,128)(2,1)} %bitcast.41), calls=%async_computation.3 | async-start | bytes 2097152 | tf_op jit(solution)/shard_map/all_to_all | solution.py:74
  164.1 104.4 %all-gather.3.cloned.1.call-start = ((), (), s32[]{:S(2)}) async-start(), calls=%async_computation.6 | async-start | bytes 1572864 | tf_op jit(solution)/shard_map/all_gather | solution.py:81
Sparse Core Ops, SparseCore 0:
  244.8 23.5 all-gather.2
where the time goes:
time: 300 us; the launch traced here: 299 us
  waiting for transfers between devices  117 us (39%)
  blocking collectives  70.7 us (24%)
  starting transfers between devices  65.6 us (22%)
  local copies, waits for them, and re-layouts  16.7 us (6%)
  between operations  14.5 us (5%)
  matrix products  11.2 us (4%)
  other arithmetic  3.49 us (1%)
    all_to_all x1, waiting for transfers between devices, summed_on_arrival(): lax.all_to_all(tiles, axis, split_axis=0, concat_axis=0, tiled=True)  55.5 us
    all_to_all x1, starting transfers between devices, sent_and_summed(): tiles = lax.all_to_all(in_blocks(shard, dim, size), axis, 0, 0, tiled=True)  44.4 us
    all_gather x1, blocking collectives, stacked_from(): tiles = lax.all_gather(tiles, axes[k], axis=0, tiled=True)  24.8 us
    all_gather x1, waiting for transfers between devices, stacked_from(): tiles = lax.all_gather(tiles, axes[k], axis=0, tiled=True)  23.7 us
    all_to_all x2, waiting for transfers between devices, from_everyone(): lax.all_to_all(jnp.broadcast_to(shard[None], (size, *shard.shape)), axis,...  21.6 us
    all_gather x1, blocking collectives, in_one_piece(): lax.all_gather(both, axis, axis=dim, tiled=True)  20.2 us
    all_to_all x2, blocking collectives, sent_and_summed(): tiles = lax.all_to_all(in_blocks(shard, dim, size), axis, 0, 0, tiled=True)  17.7 us
    all_to_all x2, starting transfers between devices, from_everyone(): lax.all_to_all(jnp.broadcast_to(shard[None], (size, *shard.shape)), axis,...  16.4 us
  transfers between devices with their start and end apart: 5, of which 5 were waited for; matrix products, arithmetic and copies ran while one was open for 2% of the time, Pallas kernels for 0%

commit v1 on v0

--- a/solution.py
+++ b/solution.py
@@ -78,7 +78,9 @@
 def stacked_from(shard, axes, order):
     tiles = shard[None]
     for k in order:
-        tiles = lax.all_gather(tiles, axes[k], axis=0, tiled=True)
+        tiles = jnp.concatenate(
+            lax.all_to_all(jnp.stack([tiles] * lax.axis_size(axes[k])), axes[k], 0, 0), axis=0
+        )
     current = [lax.axis_size(axes[k]) for k in reversed(order)]
     tiles = tiles.reshape(*current, *shard.shape)
     turned = sorted(range(len(order)), key=lambda place: order[len(order) - 1 - place])

time: 300 us -> 274 us (0.913)
  waiting for transfers between devices: 117 us -> 92.7 us
  between operations: 14.5 us -> 1.14 us
  blocking collectives: 70.7 us -> 83.7 us
    all_to_all x0 -> x2, blocking collectives: none -> 37.1 us  [stacked_from(): lax.all_to_all(jnp.stack([tiles] * lax.axis_size(axes[k])), axes[k], 0, 0)]
    all_gather x1 -> x0, blocking collectives: 24.8 us -> none  [stacked_from(): tiles = lax.all_gather(tiles, axes[k], axis=0, tiled=True)]
    all_gather x1 -> x0, waiting for transfers between devices: 23.7 us -> none  [stacked_from(): tiles = lax.all_gather(tiles, axes[k], axis=0, tiled=True)]
  transfers between devices with their start and end apart: 5 -> 4, of which waited for: 5 -> 4; matrix products, arithmetic and copies ran while one was open for 2% -> 2% of each run, Pallas kernels for 0% -> 0%
where the time goes in v1:
time: 274 us; the launch traced here: 272 us
  waiting for transfers between devices  92.7 us (34%)
  blocking collectives  83.7 us (31%)
  starting transfers between devices  65.6 us (24%)
  local copies, waits for them, and re-layouts  15.4 us (6%)
  matrix products  10.1 us (4%)
  other arithmetic  3.58 us (1%)
    all_to_all x1, waiting for transfers between devices, summed_on_arrival(): lax.all_to_all(tiles, axis, split_axis=0, concat_axis=0, tiled=True)  55.5 us
    all_to_all x1, starting transfers between devices, sent_and_summed(): tiles = lax.all_to_all(in_blocks(shard, dim, size), axis, 0, 0, tiled=True)  44.4 us
    all_to_all x2, blocking collectives, stacked_from(): lax.all_to_all(jnp.stack([tiles] * lax.axis_size(axes[k])), axes[k], 0, 0)  37.1 us
    all_to_all x2, waiting for transfers between devices, from_everyone(): lax.all_to_all(jnp.broadcast_to(shard[None], (size, *shard.shape)), axis,...  21.6 us
    all_gather x1, blocking collectives, in_one_piece(): lax.all_gather(both, axis, axis=dim, tiled=True)  20.2 us
    all_to_all x2, blocking collectives, sent_and_summed(): tiles = lax.all_to_all(in_blocks(shard, dim, size), axis, 0, 0, tiled=True)  18.4 us
    all_to_all x2, starting transfers between devices, from_everyone(): lax.all_to_all(jnp.broadcast_to(shard[None], (size, *shard.shape)), axis,...  16.4 us
    all_to_all x1, waiting for transfers between devices, sent_and_summed(): tiles = lax.all_to_all(in_blocks(shard, dim, size), axis, 0, 0, tiled=True)  15.6 us
  transfers between devices with their start and end apart: 4, of which 4 were waited for; matrix products, arithmetic and copies ran while one was open for 2% of the time, Pallas kernels for 0%

profile of v1, /device:TPU:65, one launch (start us, length us, event | category | flops | bytes accessed | tf_op | source)
XLA Modules:
  0.0 272.3 jit_solution(15488241670120172030)
XLA Ops:
  0.0 0.9 multiply_reduce_fusion.1
  1.0 0.1 concatenate.27
  1.1 0.9 fusion.11
  1.9 1.1 fusion.13
  3.1 1.2 fusion.12
  4.4 1.3 fusion.15
  5.8 0.9 fusion.14
  6.9 1.2 concatenate.25
  8.0 44.4 %all-to-all-start = ((f32[16,2,3089]{2,1,0:T(2,128)}), f32[16,2,3089]{2,1,0:T(2,128)S(1)}, u32[]{:S(2)}, u32[]{:S(2)}) async-start(f32[16,2,3089]{2,1,0:T(2,128)} %concatenate.25), calls=%async_computation | async-start | bytes 819200 | tf_op jit(solution)/shard_map/all_to_all | solution.py:22
  52.5 0.2 copy.78
  52.7 1.0 copy.64
  53.7 1.3 dynamic-slice
  55.8 0.1 fusion.30
  55.9 0.2 reduce_window_sum.11
  56.2 15.6 %all-to-all-done = f32[16,2,3089]{2,1,0:T(2,128)S(1)} async-done(((f32[16,2,3089]{2,1,0:T(2,128)}), f32[16,2,3089]{2,1,0:T(2,128)S(1)}, u32[]{:S(2)}, u32[]{:S(2)}) %all-to-all-start) | async-done | bytes 395424 | tf_op jit(solution)/shard_map/all_to_all | solution.py:22
  71.8 0.1 reduce_sum.104
  71.9 0.2 fusion.27
  72.7 0.2 fusion.35
  73.1 0.1 fusion.2
  73.3 1.7 fusion.37
  75.1 0.4 fusion.36
  75.6 0.2 multiply_reduce_fusion.2
  75.8 0.2 dynamic-update-slice
  76.1 8.0 %all-reduce = f32[4]{0:T(128)S(1)} all-reduce(f32[4]{0:T(128)S(1)} %dynamic-update-slice), channel_id=2, replica_groups=mesh['grp'=2,'dp'=8,'kv'=16,'tp'=2] {'tp'}, use_global_device_ids=true, to_apply=%add | all-reduce | flops 4 | bytes 32
  84.2 0.7 broadcast_in_dim.13
  84.9 6.0 %all-to-all-start.1 = ((bf16[16,2,1024]{2,1,0:T(2,128)(2,1)}), bf16[16,2,1024]{2,1,0:T(2,128)(2,1)S(1)}, u32[]{:S(2)}, u32[]{:S(2)}) async-start(bf16[16,2,1024]{2,1,0:T(2,128)(2,1)} %broadcast_in_dim.13), calls=%async_computation.1 | async-start | bytes 131072 | tf_op jit(solution)/shard_map/all_to_all | solution.py:42
  90.9 0.2 copy.79
  91.1 11.2 %all-to-all-done.1 = bf16[16,2,1024]{2,1,0:T(2,128)(2,1)S(1)} async-done(((bf16[16,2,1024]{2,1,0:T(2,128)(2,1)}), bf16[16,2,1024]{2,1,0:T(2,128)(2,1)S(1)}, u32[]{:S(2)}, u32[]{:S(2)}) %all-to-all-start.1) | async-done | bytes 65568 | tf_op jit(solution)/shard_map/all_to_all | solution.py:42
  102.4 0.2 convolution_bitcast_fusion
  102.6 5.5 %all_to_all.41 = f32[2,32,128]{2,1,0:T(8,128)S(1)} all-to-all(f32[2,32,128]{2,1,0:T(8,128)S(1)} %convolution_bitcast_fusion), channel_id=1, replica_groups=mesh['grp'=2,'dp'=8,'kv'=16,'tp'=2] {'tp'}, dimensions={0} | all-to-all | bytes 65536 | tf_op jit(solution)/shard_map/all_to_all | solution.py:22
  108.1 20.2 %all_gather.11 = bf16[256,256]{1,0:T(8,128)(2,1)S(1)} all-gather(bf16[32,256]{1,0:T(8,128)(2,1)S(1)} %pad_maximum_fusion.1), channel_id=1, replica_groups=mesh['grp'=2,'dp'=8,'kv'=16,'tp'=2] {'dp'}, dimensions={0}, use_global_device_ids=true | all-gather | bytes 147456 | tf_op jit(solution)/shard_map/all_gather | solution.py:64
  128.3 0.1 multiply_reduce_fusion
  128.4 0.6 broadcast_in_dim.14
  129.1 10.4 %all-to-all-start.4 = ((f32[32,1,256]{2,1,0:T(1,128)}), f32[32,1,256]{2,1,0:T(1,128)S(1)}, u32[]{:S(2)}, u32[]{:S(2)}) async-start(f32[32,1,256]{2,1,0:T(1,128)} %broadcast_in_dim.14), calls=%async_computation.4 | async-start | bytes 65536 | tf_op jit(solution)/shard_map/all_to_all | solution.py:42
  139.5 0.4 convolution_convert_fusion
  139.9 1.3 copy.66
  141.2 10.4 %all-to-all-done.4 = f32[32,1,256]{2,1,0:T(1,128)S(1)} async-done(((f32[32,1,256]{2,1,0:T(1,128)}), f32[32,1,256]{2,1,0:T(1,128)S(1)}, u32[]{:S(2)}, u32[]{:S(2)}) %all-to-all-start.4) | async-done | bytes 32800 | tf_op jit(solution)/shard_map/all_to_all | solution.py:42
  151.6 4.8 %all-to-all-start.3 = ((bf16[32,256,64]{1,2,0:T(8,128)(2,1)}), bf16[32,256,64]{1,2,0:T(8,128)(2,1)S(1)}, u32[]{:S(2)}, u32[]{:S(2)}) async-start(bf16[32,256,64]{1,2,0:T(8,128)(2,1)} %bitcast.41), calls=%async_computation.3 | async-start | bytes 2097152 | tf_op jit(solution)/shard_map/all_to_all | solution.py:74
  156.5 55.5 %all-to-all-done.3 = bf16[32,256,64]{1,2,0:T(8,128)(2,1)S(1)} async-done(((bf16[32,256,64]{1,2,0:T(8,128)(2,1)}), bf16[32,256,64]{1,2,0:T(8,128)(2,1)S(1)}, u32[]{:S(2)}, u32[]{:S(2)}) %all-to-all-start.3) | async-done | bytes 1048608 | tf_op jit(solution)/shard_map/all_to_all | solution.py:74
  212.1 0.2 convert_reduce_fusion
  212.3 26.1 %all_to_all.42 = bf16[16,1,256,64]{2,3,1,0:T(8,128)(2,1)S(1)} all-to-all(bf16[16,1,256,64]{2,3,1,0:T(8,128)(2,1)S(1)} %stack.6), channel_id=1, replica_groups=mesh['grp'=2,'dp'=8,'kv'=16,'tp'=2] {'kv'}, dimensions={0} | all-to-all | bytes 1048576 | tf_op jit(solution)/shard_map/all_to_all | solution.py:82
  238.5 11.0 %all_to_all.43 = bf16[2,16,256,64]{2,3,1,0:T(8,128)(2,1)S(1)} all-to-all(bf16[2,16,256,64]{2,3,1,0:T(8,128)(2,1)S(1)} %pad_maximum_fusion), channel_id=1, replica_groups=mesh['grp'=2,'dp'=8,'kv'=16,'tp'=2] {'tp'}, dimensions={0} | all-to-all | bytes 2097152 | tf_op jit(solution)/shard_map/all_to_all | solution.py:82
  249.5 1.1 copy.68
  250.5 3.9 %copy.69 = bf16[256,32,64]{2,1,0:T(8,128)(2,1)S(1)} copy(bf16[256,32,64]{0,2,1:T(8,128)(2,1)} %bitcast.92) | data formatting | bytes 2097152 | tf_op jit(solution)/shard_map/transpose | solution.py:50
  254.5 2.4 dot_general.51
  256.9 1.8 fusion
  258.7 13.0 %all_to_all.44 = f32[8,32,128]{2,1,0:T(8,128)S(1)} all-to-all(f32[8,32,128]{2,1,0:T(8,128)S(1)} %fusion), channel_id=1, replica_groups=mesh['grp'=2,'dp'=8,'kv'=16,'tp'=2] {'dp'}, dimensions={0} | all-to-all | bytes 262144 | tf_op jit(solution)/shard_map/all_to_all | solution.py:22
  271.7 0.6 fusion.5
  (83 shorter events, 2.0 us)
Async XLA Ops:
  0.0 73.3 %copy-start = (f32[2,16,64,128]{3,2,1,0:T(8,128)S(1)}, f32[2,16,64,128]{3,2,1,0:T(8,128)}, u32[]{:S(2)}) copy-start(f32[2,16,64,128]{3,2,1,0:T(8,128)} %param.44) | copy-start | bytes 3145732
  0.0 5.8 %copy-start.3 = (bf16[256,1024]{1,0:T(8,128)(2,1)S(1)}, bf16[256,1024]{1,0:T(8,128)(2,1)}, u32[]{:S(2)}) copy-start(bf16[256,1024]{1,0:T(8,128)(2,1)} %param.28) | copy-start | bytes 1572868
  3.1 49.4 %copy-start.8 = (f32[2,128,16]{1,2,0:T(8,128)S(1)}, f32[2,128,16]{1,2,0:T(8,128)}, u32[]{:S(2)}) copy-start(f32[2,128,16]{1,2,0:T(8,128)} %param.42) | copy-start | bytes 49156
  3.1 49.4 %copy-start.7 = (bf16[2,128,512]{2,1,0:T(8,128)(2,1)S(1)}, bf16[2,128,512]{2,1,0:T(8,128)(2,1)}, u32[]{:S(2)}) copy-start(bf16[2,128,512]{2,1,0:T(8,128)(2,1)} %param.41) | copy-start | bytes 786436
  4.3 48.4 %copy-start.4 = (bf16[2,128,1024]{2,1,0:T(8,128)(2,1)S(1)}, bf16[2,128,1024]{2,1,0:T(8,128)(2,1)}, u32[]{:S(2)}) copy-start(bf16[2,128,1024]{2,1,0:T(8,128)(2,1)} %param.40) | copy-start | bytes 1572868
  5.8 49.9 %copy-start.18 = (s32[2]{0:T(128)S(1)}, s32[2]{0:T(128)}, u32[]{:S(2)}) copy-start(s32[2]{0:T(128)} %param.43) | copy-start | bytes 28
  6.7 49.4 %copy-start.19 = (f32[16]{0:T(128)S(1)}, f32[16]{0:T(128)}, u32[]{:S(2)}) copy-start(f32[16]{0:T(128)} %param.39) | copy-start | bytes 196
  6.7 49.4 %copy-start.11 = (f32[4,512]{1,0:T(4,128)S(1)}, f32[4,512]{1,0:T(4,128)}, u32[]{:S(2)}) copy-start(f32[4,512]{1,0:T(4,128)} %param.33) | copy-start | bytes 24580
  6.7 49.4 %copy-start.12 = (f32[4,512]{1,0:T(4,128)S(1)}, f32[4,512]{1,0:T(4,128)}, u32[]{:S(2)}) copy-start(f32[4,512]{1,0:T(4,128)} %param.34) | copy-start | bytes 24580
  6.8 49.4 %copy-start.9 = (f32[4,1024]{1,0:T(4,128)S(1)}, f32[4,1024]{1,0:T(4,128)}, u32[]{:S(2)}) copy-start(f32[4,1024]{1,0:T(4,128)} %param.32) | copy-start | bytes 49156
  6.8 65.2 %copy-start.13 = (bf16[2,3,512]{2,0,1:T(2,128)(2,1)S(1)}, bf16[2,3,512]{2,0,1:T(2,128)(2,1)}, u32[]{:S(2)}) copy-start(bf16[2,3,512]{2,0,1:T(2,128)(2,1)} %param.37) | copy-start | bytes 18436
  6.9 65.2 %copy-start.14 = (bf16[2,3,512]{2,0,1:T(2,128)(2,1)S(1)}, bf16[2,3,512]{2,0,1:T(2,128)(2,1)}, u32[]{:S(2)}) copy-start(bf16[2,3,512]{2,0,1:T(2,128)(2,1)} %param.36) | copy-start | bytes 18436
  6.9 65.6 %copy-start.10 = (bf16[2,3,1024]{2,0,1:T(2,128)(2,1)S(1)}, bf16[2,3,1024]{2,0,1:T(2,128)(2,1)}, u32[]{:S(2)}) copy-start(bf16[2,3,1024]{2,0,1:T(2,128)(2,1)} %param.35) | copy-start | bytes 36868
  8.0 64.9 %copy-start.17 = (f32[16]{0:T(128)S(1)}, f32[16]{0:T(128)}, u32[]{:S(2)}) copy-start(f32[16]{0:T(128)} %param.38) | copy-start | bytes 196
  8.0 63.7 %all-to-all-start = ((f32[16,2,3089]{2,1,0:T(2,128)}), f32[16,2,3089]{2,1,0:T(2,128)S(1)}, u32[]{:S(2)}, u32[]{:S(2)}) async-start(f32[16,2,3089]{2,1,0:T(2,128)} %concatenate.25), calls=%async_computation | async-start | bytes 819200 | tf_op jit(solution)/shard_map/all_to_all | solution.py:22
  53.7 21.4 %copy-start.6 = (bf16[2,128,1024]{1,2,0:T(8,128)(2,1)S(1)}, bf16[2,128,1024]{1,2,0:T(8,128)(2,1)}, u32[]{:S(2)}) copy-start(bf16[2,128,1024]{1,2,0:T(8,128)(2,1)} %copy.64) | copy-start | bytes 1572868
  53.7 30.5 %copy-start.15 = (f32[1024]{0:T(1024)S(1)}, f32[1024]{0:T(1024)}, u32[]{:S(2)}) copy-start(f32[1024]{0:T(1024)} %param.45) | copy-start | bytes 12292
  55.8 35.1 %copy-start.1 = (bf16[32,256]{1,0:T(8,128)(2,1)S(1)}, bf16[32,256]{1,0:T(8,128)(2,1)}, u32[]{:S(2)}) copy-start(bf16[32,256]{1,0:T(8,128)(2,1)} %param.25) | copy-start | bytes 49156
  55.9 35.0 %copy-start.5 = (bf16[1024,256]{1,0:T(8,128)(2,1)S(1)}, bf16[1024,256]{1,0:T(8,128)(2,1)}, u32[]{:S(2)}) copy-start(bf16[1024,256]{1,0:T(8,128)(2,1)} %param.46) | copy-start | bytes 1572868
  73.2 34.9 %copy-start.16 = (f32[128]{0:T(128)S(1)}, f32[128]{0:T(128)}, u32[]{:S(2)}) copy-start(f32[128]{0:T(128)} %param.47) | copy-start | bytes 1540
  73.3 66.1 %copy-start.2 = (bf16[128,2048]{1,0:T(8,128)(2,1)S(1)}, bf16[128,2048]{1,0:T(8,128)(2,1)}, u32[]{:S(2)}) copy-start(bf16[128,2048]{1,0:T(8,128)(2,1)} %param.48) | copy-start | bytes 1572868
  84.9 17.4 %all-to-all-start.1 = ((bf16[16,2,1024]{2,1,0:T(2,128)(2,1)}), bf16[16,2,1024]{2,1,0:T(2,128)(2,1)S(1)}, u32[]{:S(2)}, u32[]{:S(2)}) async-start(bf16[16,2,1024]{2,1,0:T(2,128)(2,1)} %broadcast_in_dim.13), calls=%async_computation.1 | async-start | bytes 131072 | tf_op jit(solution)/shard_map/all_to_all | solution.py:42
  129.1 22.6 %all-to-all-start.4 = ((f32[32,1,256]{2,1,0:T(1,128)}), f32[32,1,256]{2,1,0:T(1,128)S(1)}, u32[]{:S(2)}, u32[]{:S(2)}) async-start(f32[32,1,256]{2,1,0:T(1,128)} %broadcast_in_dim.14), calls=%async_computation.4 | async-start | bytes 65536 | tf_op jit(solution)/shard_map/all_to_all | solution.py:42
  151.6 60.5 %all-to-all-start.3 = ((bf16[32,256,64]{1,2,0:T(8,128)(2,1)}), bf16[32,256,64]{1,2,0:T(8,128)(2,1)S(1)}, u32[]{:S(2)}, u32[]{:S(2)}) async-start(bf16[32,256,64]{1,2,0:T(8,128)(2,1)} %bitcast.41), calls=%async_computation.3 | async-start | bytes 2097152 | tf_op jit(solution)/shard_map/all_to_all | solution.py:74
